TPU v7x, 128 devices: a whole 4x4x4 slice. The times are simulated.
128 devices in a mesh: sp: 16 (over z, y), dp: 8 (over x, core).
Axes of the slice: x: 4, y: 4, z: 4, core: 2. Of those that a mesh axis runs over, the one named last changes fastest.
Arguments:
- tokens: bfloat16 [8, 4096, 2048], P('dp', 'sp'), may hold values from -6 to 6
- in_gain: float32 [2048], replicated, may hold values from 0.1 to 1.9
- w_query_down: bfloat16 [2048, 512], P('dp'), may hold values from -0.125 to 0.125
- w_latent_down: bfloat16 [2048, 256], P('dp'), may hold values from -0.125 to 0.125
- w_rope_key: bfloat16 [2048, 64], replicated, may hold values from -0.125 to 0.125
- query_latent_gain: float32 [512], replicated, may hold values from 0.1 to 1.9
- latent_gain: float32 [256], replicated, may hold values from 0.1 to 1.9
- w_query_up: bfloat16 [512, 3072], P('dp', 'sp'), may hold values from -0.25 to 0.25
- w_key_up: bfloat16 [256, 2048], P('dp', 'sp'), may hold values from -0.375 to 0.375
- w_value_up: bfloat16 [256, 2048], P('dp', 'sp'), may hold values from -0.375 to 0.375
- query_gain: float32 [192], replicated, may hold values from 0.5 to 14
- key_gain: float32 [192], replicated, may hold values from 0.5 to 14
- out_gain: float32 [2048], replicated, may hold values from 0.1 to 1.9
- w_out: bfloat16 [2048, 2048], P(('sp', 'dp')), may hold values from -0.125 to 0.125
Outputs:
- result: bfloat16 [8, 4096, 2048], P('dp', 'sp')
All inputs are finite; a program needn't handle non-finite values.
Results may differ from a plain program's by a relative error of at most 0.034.
The roundings to bfloat16 on the way count: a program that leaves them out, or rounds other values in their place, can miss the bound.
Values may be sent and summed in bfloat16 or wider, within the bound.
No kernel may reach another device: no remote copies, remote signals or barrier semaphores. Data moves between devices by JAX's collectives and lax.ppermute only.
A program may use at most 64 MiB of HBM per device.

v0:
```python
import jax
import jax.numpy as jnp
from jax import lax
from jax.sharding import PartitionSpec as P

HEADS = 16
EPS = 1e-06
THETA = 10000.0
NEG_BIG = -1e30


def in_one_piece(arrays, axis, dim, along):
    ends, at = ([], 0)
    for a in arrays[:-1]:
        at += a.shape[along]
        ends.append(at)
    both = jnp.concatenate(arrays, axis=along)
    return tuple(jnp.split(lax.all_gather(both, axis, axis=dim, tiled=True), ends, axis=along))


def joined_along(blocks, dim):
    dims = list(blocks.shape[1:])
    dims[dim] *= blocks.shape[0]
    return jnp.moveaxis(blocks, 0, dim).reshape(dims)


def sent_to_all(value, axis):
    copies = jnp.broadcast_to(value, (lax.axis_size(axis), *value.shape))
    return lax.all_to_all(copies, axis, split_axis=0, concat_axis=0, tiled=True)


def gathered_copies(value, axis, dim):
    return joined_along(sent_to_all(value, axis), dim)


def rms_scale(values, scaling):
    return values * lax.rsqrt(jnp.mean(values * values, axis=-1, keepdims=True) + EPS) * scaling


def rotate(tail_part, positions):
    half_width = tail_part.shape[-1] // 2
    frequency = THETA ** (-jnp.arange(half_width, dtype=jnp.float32) / half_width)
    angles = positions[:, None] * frequency[None, :]
    cosine = jnp.cos(angles)[:, None, :]
    sine = jnp.sin(angles)[:, None, :]
    first_half = tail_part[..., :half_width]
    second_half = tail_part[..., half_width:]
    return jnp.concatenate(
        [first_half * cosine - second_half * sine, second_half * cosine + first_half * sine],
        axis=-1,
    )


def finish_heads(joined, positions, scaling, rope_width):
    row_count = joined.shape[0]
    normal = rms_scale(joined, scaling)
    turned = rotate(normal[..., -rope_width:], positions)
    return (
        jnp.concatenate([normal[..., :-rope_width], turned], axis=-1)
        .astype(jnp.bfloat16)
        .reshape(row_count, -1)
    )


def make_queries(query_total, positions, scaling, head_count, rope_width):
    row_count = query_total.shape[0]
    return finish_heads(
        query_total.reshape(row_count, head_count, -1), positions, scaling, rope_width
    )


def make_keys(key_total, rope_key, positions, scaling, head_count):
    row_count = key_total.shape[0]
    rope_width = rope_key.shape[1]
    shaped = key_total.reshape(row_count, head_count, -1)
    shared = rope_key.astype(jnp.float32)[:, None, :]
    return finish_heads(jnp.concatenate([shaped, shared], axis=-1), positions, scaling, rope_width)


def single_fold(inputs, piece):
    return jnp.dot(inputs, piece, preferred_element_type=jnp.float32)


def double_fold(inputs, pieces):
    return (
        jnp.dot(inputs, pieces[0], preferred_element_type=jnp.float32),
        jnp.dot(inputs, pieces[1], preferred_element_type=jnp.float32),
    )


def attend(queries, keys, values, head_count):
    length = queries.shape[0]
    block_rows = min(512, length)
    query_blocks = queries.reshape(length // block_rows, block_rows, head_count, -1)
    key_heads = keys.reshape(length, head_count, -1)
    value_heads = values.reshape(length, head_count, -1)
    score_scale = key_heads.shape[-1] ** (-0.5)
    key_pos = jnp.arange(length)

    def one_block(block_args):
        query_block, block_index = block_args
        scores = (
            jnp.einsum("qhd,khd->hqk", query_block, key_heads, preferred_element_type=jnp.float32)
            * score_scale
        )
        query_pos = block_index * block_rows + jnp.arange(block_rows)
        allowed = key_pos[None, :] <= query_pos[:, None]
        scores = jnp.where(allowed[None], scores, NEG_BIG)
        weights = jax.nn.softmax(scores, axis=-1).astype(jnp.bfloat16)
        return jnp.einsum(
            "hqk,khd->qhd", weights, value_heads, preferred_element_type=jnp.float32
        ).astype(jnp.bfloat16)

    outcome = lax.map(one_block, (query_blocks, jnp.arange(length // block_rows)))
    return outcome.reshape(length, -1)


def per_device(
    tokens,
    in_gain,
    w_query_down,
    w_latent_down,
    w_rope_key,
    query_latent_gain,
    latent_gain,
    w_query_up,
    w_key_up,
    w_value_up,
    query_gain,
    key_gain,
    out_gain,
    w_out,
):
    seq_devices = lax.axis_size("sp")
    head_count = HEADS // seq_devices
    own_rows = tokens.shape[1]
    length = own_rows * seq_devices
    rope_width = w_rope_key.shape[1]
    local_rows = tokens.reshape(own_rows, tokens.shape[2])
    normed = rms_scale(local_rows.astype(jnp.float32), in_gain).astype(jnp.bfloat16)
    query_sum, latent_sum = double_fold(
        normed, in_one_piece((w_query_down, w_latent_down), "dp", 0, 1)
    )
    latent_q = rms_scale(query_sum, query_latent_gain).astype(jnp.bfloat16)
    latent_kv = rms_scale(latent_sum, latent_gain).astype(jnp.bfloat16)
    rope_key = jnp.dot(normed, w_rope_key, preferred_element_type=jnp.float32).astype(jnp.bfloat16)
    every_q, every_kv, every_rope = in_one_piece((latent_q, latent_kv, rope_key), "sp", 0, 1)
    positions = jnp.arange(length, dtype=jnp.float32)
    query_total = single_fold(every_q, gathered_copies(w_query_up, "dp", 0))
    key_total, value_total = double_fold(
        every_kv,
        (
            lax.all_gather(w_key_up, "dp", axis=0, tiled=True),
            lax.all_gather(w_value_up, "dp", axis=0, tiled=True),
        ),
    )
    queries = make_queries(query_total, positions, query_gain, head_count, rope_width)
    keys = make_keys(key_total, every_rope, positions, key_gain, head_count)
    values = value_total.astype(jnp.bfloat16)
    attended = attend(queries, keys, values, head_count)
    token_heads = lax.all_to_all(attended, "sp", split_axis=0, concat_axis=1, tiled=True)
    mixed = rms_scale(token_heads.astype(jnp.float32), out_gain).astype(jnp.bfloat16)
    projected = single_fold(mixed, lax.all_gather(w_out, ("sp", "dp"), axis=0, tiled=True))
    return projected.astype(jnp.bfloat16).reshape(1, own_rows, w_out.shape[1])


def solution(mesh):
    in_specs = (
        P("dp", "sp", None),
        P(),
        P("dp", None),
        P("dp", None),
        P(),
        P(),
        P(),
        P("dp", "sp"),
        P("dp", "sp"),
        P("dp", "sp"),
        P(),
        P(),
        P(),
        P(("sp", "dp"), None),
    )
    out_specs = P("dp", "sp", None)
    return jax.shard_map(
        per_device, mesh=mesh, in_specs=in_specs, out_specs=out_specs, check_vma=False
    )
```

profile of v0, /device:TPU:0, one launch (start us, length us, event | category | flops | bytes accessed | tf_op | source)
XLA Modules:
  0.0 225.6 jit_solution(16825096950358641469)
XLA Ops:
  6.5 1.9 pad_maximum_fusion.4
  8.5 1.5 fusion.17
  10.0 1.7 convolution_convert_fusion.2
  11.8 0.1 copy.37
  11.9 27.3 %all-gather.4.cloned.1.call-done = bf16[2048,768]{1,0:T(8,128)(2,1)} async-done(((bf16[256,768]{1,0:T(8,128)(2,1)}), bf16[2048,768]{1,0:T(8,128)(2,1)}) %all-gather.4.cloned.1.call-update) | async-done | bytes 3145744 | tf_op jit(solution)/shard_map/all_gather | solution.py:18
  39.2 2.4 %multiply_reduce_fusion.2 = (f32[256]{0:T(256)S(1)}, f32[256,512]{1,0:T(8,128)S(1)}) fusion(bf16[2048,768]{1,0:T(8,128)(2,1)} %all-gather.4.cloned.1.call-done, bf16[1,256,2048]{2,1,0:T(8,128)(2,1)S(1)} %copy-done.2, f32[2048]{0:T(1024)S(1)} %copy-done.11, f32[256]{0:T(256)S(1)} %add_rsqrt_fusion.5), kind=kOutput, calls=%fused_computation.61 | convolution fusion | flops 539229952 | bytes 3680256 | tf_op jit(solution)/shard_map/dot_general | solution.py:86
  41.7 1.9 multiply_reduce_fusion.3
  43.6 0.1 copy.36
  44.0 0.8 pad_maximum_fusion.3
  44.8 0.7 broadcast_in_dim.11
  45.6 4.0 %all-to-all-start = ((bf16[8,64,192]{2,1,0:T(8,128)(2,1)}), bf16[8,64,192]{2,1,0:T(8,128)(2,1)}, u32[]{:S(2)}, u32[]{:S(2)}) async-start(bf16[8,64,192]{2,1,0:T(8,128)(2,1)} %broadcast_in_dim.11), calls=%async_computation | async-start | bytes 524288 | tf_op jit(solution)/shard_map/all_to_all | solution.py:29
  49.7 0.7 all-gather.8.cloned.1.call-update
  50.4 13.8 %all_gather.17 = bf16[256,128]{1,0:T(8,128)(2,1)S(1)} all-gather(bf16[32,128]{1,0:T(8,128)(2,1)S(1)} %copy-done.5), channel_id=1, replica_groups=mesh['sp'=16,'dp'=8] {'dp'}, dimensions={0}, use_global_device_ids=true | all-gather | bytes 73728 | tf_op jit(solution)/shard_map/all_gather | solution.py:153
  64.2 12.9 %all_gather.18 = bf16[256,128]{1,0:T(8,128)(2,1)S(1)} all-gather(bf16[32,128]{1,0:T(8,128)(2,1)S(1)} %copy-done.6), channel_id=1, replica_groups=mesh['sp'=16,'dp'=8] {'dp'}, dimensions={0}, use_global_device_ids=true | all-gather | bytes 73728 | tf_op jit(solution)/shard_map/all_gather | solution.py:154
  77.1 34.1 %all-gather.6.cloned.1.call-done = bf16[4096,832]{1,0:T(8,128)(2,1)} async-done(((bf16[256,832]{1,0:T(8,128)(2,1)}), bf16[4096,832]{1,0:T(8,128)(2,1)}) %all-gather.6.cloned.1.call-update) | async-done | bytes 6815760 | tf_op jit(solution)/shard_map/all_gather | solution.py:18
  111.2 1.4 fusion.26
  112.5 0.6 copy.41
  113.1 2.4 %convolution_bitcast_fusion = f32[4096,1,128]{0,2,1:T(8,128)S(1)} fusion(bf16[256,128]{1,0:T(8,128)(2,1)S(1)} %all_gather.17, bf16[4096,832]{1,0:T(8,128)(2,1)} %all-gather.6.cloned.1.call-done), kind=kOutput, calls=%fused_computation.16 | convolution fusion | flops 268435456 | bytes 4259840 | tf_op jit(solution)/shard_map/dot_general | solution.py:86
  115.5 0.3 multiply_reduce_fusion
  115.8 3.8 %multiply_reduce_fusion.1 = (f32[4096]{0:T(1024)S(1)}, f32[4096,192]{0,1:T(8,128)S(1)}) fusion(bf16[512,192]{1,0:T(8,128)(2,1)} %bitcast.2, bf16[4096,832]{1,0:T(8,128)(2,1)} %all-gather.6.cloned.1.call-done), kind=kOutput, calls=%fused_computation.25 | convolution fusion | flops 806875136 | bytes 7618560 | tf_op jit(solution)/shard_map/dot_general | solution.py:81
  119.6 0.5 multiply_multiply_fusion
  120.3 0.5 multiply_bitcast_fusion
  120.9 2.5 %subtract_convert_fusion = (bf16[4096,1,32]{0,2,1:T(8,128)(2,1)S(1)}, bf16[4096,1,32]{0,2,1:T(8,128)(2,1)S(1)}, bf16[4096,1,32]{0,2,1:T(8,128)(2,1)S(1)}, bf16[4096,1,32]{0,2,1:T(8,128)(2,1)S(1)}) fusion(f32[4096,1,192]{0,2,1:T(8,128)S(1)} %multiply_multiply_fusion, f32[32]{0:T(128)S(1)} %multiply_power_fusion, f32[4096,1,192]{0,2,1:T(8,128)S(1)} %multiply_bitcast_fusion), kind=kLoop, calls=%fused_computation.54 | loop fusion | flops 2228224 | bytes 3145856 | tf_op jit(solution)/shard_map/convert.5
  123.6 0.1 pad_maximum_fusion.2
  123.9 3.3 %fusion.12 = bf16[4096,1,128]{2,0,1:T(8,128)(2,1)} fusion(bf16[256,128]{1,0:T(8,128)(2,1)S(1)} %all_gather.18, bf16[4096,832]{1,0:T(8,128)(2,1)} %all-gather.6.cloned.1.call-done), kind=kOutput, calls=%fused_computation.18 | convolution fusion | flops 268959744 | bytes 3211264 | tf_op jit(solution)/shard_map/dot_general | solution.py:87
  127.2 58.7 %while.11 = (s32[]{:T(128)}, bf16[8,512,1,128]{3,1,2,0:T(8,128)(2,1)}, s32[8]{0:T(128)S(1)}, bf16[8,512,1,192]{1,3,2,0:T(8,128)(2,1)S(1)}, bf16[4096,1,192]{0,2,...) while((s32[]{:T(128)}, bf16[8,512,1,128]{3,1,2,0:T(8,128)(2,1)}, ...), condition=%wide.region_8.9_spmd.clone, body=%wide.region_5.8_spmd.clone.sunk | while | flops 1361116672 | bytes 32324240 | solution.py:114
  127.2 0.6 dynamic_slice.19
  128.5 1.9 fusion.46
  130.4 1.3 fusion.47
  131.7 2.8 %fusion.48 = bf16[8,512,1,128]{3,1,2,0:T(8,128)(2,1)} fusion(bf16[8,512,1,128]{3,1,2,0:T(8,128)(2,1)} %get-tuple-element.141, s32[]{:T(128)} %get-tuple-element.140, f32[512,4096]{1,0:T(8,128)S(1)} %get-tuple-element.130, f32[512]{0:T(512)S(1)} %fusion.47, f32[512]{0:T(512)S(1)} %get-tuple-element.131, bf16[4096,1,128]{2,0,1:T(8,128)(2,1)S(1)} %copy-done.1), kind=kOutput, calls=%fused_computation.10.clone.1 | convolution fusion | flops 543227904 | bytes 9572864 | tf_op jit(solution)/shard_map/while/body/eval_jaxpr/hqk,khd->qhd/dot_general | solution.py:110
  134.5 0.6 dynamic_slice.19
  135.8 2.0 fusion.46
  137.8 1.3 fusion.47
  139.0 2.8 %fusion.48 = bf16[8,512,1,128]{3,1,2,0:T(8,128)(2,1)} fusion(bf16[8,512,1,128]{3,1,2,0:T(8,128)(2,1)} %get-tuple-element.141, s32[]{:T(128)} %get-tuple-element.140, f32[512,4096]{1,0:T(8,128)S(1)} %get-tuple-element.130, f32[512]{0:T(512)S(1)} %fusion.47, f32[512]{0:T(512)S(1)} %get-tuple-element.131, bf16[4096,1,128]{2,0,1:T(8,128)(2,1)S(1)} %copy-done.1), kind=kOutput, calls=%fused_computation.10.clone.1 | convolution fusion | flops 543227904 | bytes 9572864 | tf_op jit(solution)/shard_map/while/body/eval_jaxpr/hqk,khd->qhd/dot_general | solution.py:110
  141.9 0.6 dynamic_slice.19
  143.1 2.0 fusion.46
  145.1 1.3 fusion.47
  146.4 2.8 %fusion.48 = bf16[8,512,1,128]{3,1,2,0:T(8,128)(2,1)} fusion(bf16[8,512,1,128]{3,1,2,0:T(8,128)(2,1)} %get-tuple-element.141, s32[]{:T(128)} %get-tuple-element.140, f32[512,4096]{1,0:T(8,128)S(1)} %get-tuple-element.130, f32[512]{0:T(512)S(1)} %fusion.47, f32[512]{0:T(512)S(1)} %get-tuple-element.131, bf16[4096,1,128]{2,0,1:T(8,128)(2,1)S(1)} %copy-done.1), kind=kOutput, calls=%fused_computation.10.clone.1 | convolution fusion | flops 543227904 | bytes 9572864 | tf_op jit(solution)/shard_map/while/body/eval_jaxpr/hqk,khd->qhd/dot_general | solution.py:110
  149.2 0.6 dynamic_slice.19
  150.5 2.0 fusion.46
  152.4 1.3 fusion.47
  153.7 2.8 %fusion.48 = bf16[8,512,1,128]{3,1,2,0:T(8,128)(2,1)} fusion(bf16[8,512,1,128]{3,1,2,0:T(8,128)(2,1)} %get-tuple-element.141, s32[]{:T(128)} %get-tuple-element.140, f32[512,4096]{1,0:T(8,128)S(1)} %get-tuple-element.130, f32[512]{0:T(512)S(1)} %fusion.47, f32[512]{0:T(512)S(1)} %get-tuple-element.131, bf16[4096,1,128]{2,0,1:T(8,128)(2,1)S(1)} %copy-done.1), kind=kOutput, calls=%fused_computation.10.clone.1 | convolution fusion | flops 543227904 | bytes 9572864 | tf_op jit(solution)/shard_map/while/body/eval_jaxpr/hqk,khd->qhd/dot_general | solution.py:110
  156.5 0.6 dynamic_slice.19
  157.8 2.0 fusion.46
  159.8 1.3 fusion.47
  161.0 2.8 %fusion.48 = bf16[8,512,1,128]{3,1,2,0:T(8,128)(2,1)} fusion(bf16[8,512,1,128]{3,1,2,0:T(8,128)(2,1)} %get-tuple-element.141, s32[]{:T(128)} %get-tuple-element.140, f32[512,4096]{1,0:T(8,128)S(1)} %get-tuple-element.130, f32[512]{0:T(512)S(1)} %fusion.47, f32[512]{0:T(512)S(1)} %get-tuple-element.131, bf16[4096,1,128]{2,0,1:T(8,128)(2,1)S(1)} %copy-done.1), kind=kOutput, calls=%fused_computation.10.clone.1 | convolution fusion | flops 543227904 | bytes 9572864 | tf_op jit(solution)/shard_map/while/body/eval_jaxpr/hqk,khd->qhd/dot_general | solution.py:110
  163.9 0.6 dynamic_slice.19
  165.1 2.0 fusion.46
  167.1 1.3 fusion.47
  168.4 2.8 %fusion.48 = bf16[8,512,1,128]{3,1,2,0:T(8,128)(2,1)} fusion(bf16[8,512,1,128]{3,1,2,0:T(8,128)(2,1)} %get-tuple-element.141, s32[]{:T(128)} %get-tuple-element.140, f32[512,4096]{1,0:T(8,128)S(1)} %get-tuple-element.130, f32[512]{0:T(512)S(1)} %fusion.47, f32[512]{0:T(512)S(1)} %get-tuple-element.131, bf16[4096,1,128]{2,0,1:T(8,128)(2,1)S(1)} %copy-done.1), kind=kOutput, calls=%fused_computation.10.clone.1 | convolution fusion | flops 543227904 | bytes 9572864 | tf_op jit(solution)/shard_map/while/body/eval_jaxpr/hqk,khd->qhd/dot_general | solution.py:110
  171.2 0.6 dynamic_slice.19
  172.5 2.0 fusion.46
  174.4 1.3 fusion.47
  175.8 2.8 %fusion.48 = bf16[8,512,1,128]{3,1,2,0:T(8,128)(2,1)} fusion(bf16[8,512,1,128]{3,1,2,0:T(8,128)(2,1)} %get-tuple-element.141, s32[]{:T(128)} %get-tuple-element.140, f32[512,4096]{1,0:T(8,128)S(1)} %get-tuple-element.130, f32[512]{0:T(512)S(1)} %fusion.47, f32[512]{0:T(512)S(1)} %get-tuple-element.131, bf16[4096,1,128]{2,0,1:T(8,128)(2,1)S(1)} %copy-done.1), kind=kOutput, calls=%fused_computation.10.clone.1 | convolution fusion | flops 543227904 | bytes 9572864 | tf_op jit(solution)/shard_map/while/body/eval_jaxpr/hqk,khd->qhd/dot_general | solution.py:110
  178.6 0.6 dynamic_slice.19
  179.9 1.9 fusion.46
  181.8 1.3 fusion.47
  183.1 2.8 %fusion.48 = bf16[8,512,1,128]{3,1,2,0:T(8,128)(2,1)} fusion(bf16[8,512,1,128]{3,1,2,0:T(8,128)(2,1)} %get-tuple-element.141, s32[]{:T(128)} %get-tuple-element.140, f32[512,4096]{1,0:T(8,128)S(1)} %get-tuple-element.130, f32[512]{0:T(512)S(1)} %fusion.47, f32[512]{0:T(512)S(1)} %get-tuple-element.131, bf16[4096,1,128]{2,0,1:T(8,128)(2,1)S(1)} %copy-done.1), kind=kOutput, calls=%fused_computation.10.clone.1 | convolution fusion | flops 543227904 | bytes 9572864 | tf_op jit(solution)/shard_map/while/body/eval_jaxpr/hqk,khd->qhd/dot_general | solution.py:110
  185.9 22.2 %all_to_all.18 = bf16[16,256,128]{2,1,0:T(8,128)(2,1)S(1)} all-to-all(bf16[16,256,128]{2,1,0:T(8,128)(2,1)} %bitcast.7), channel_id=1, replica_groups=mesh['sp'=16,'dp'=8] {'sp'}, dimensions={0} | all-to-all | bytes 2097152 | tf_op jit(solution)/shard_map/all_to_all | solution.py:161
  208.2 1.6 convert_bitcast_fusion
  209.7 1.9 copy.42
  211.7 0.3 fusion.16
  212.0 0.3 fusion.23
  212.4 6.7 %fusion.15 = bf16[1,256,2048]{2,1,0:T(8,128)(2,1)} fusion(bf16[256,2048]{0,1:T(8,128)(2,1)S(1)} %fusion.23, bf16[2048,2048]{1,0:T(8,128)(2,1)} %all-gather.8.cloned.1.call-done), kind=kOutput, calls=%fused_computation.31 | convolution fusion | flops 2148007936 | bytes 10485760 | tf_op jit(solution)/shard_map/dot_general | solution.py:81
  (69 shorter events, 1.1 us)
Async XLA Ops:
  6.5 3.5 %copy-start = (bf16[2048,64]{0,1:T(8,128)(2,1)S(1)}, bf16[2048,64]{0,1:T(8,128)(2,1)}, u32[]{:S(2)}) copy-start(bf16[2048,64]{0,1:T(8,128)(2,1)} %param.20) | copy-start | bytes 786436
  6.5 32.7 %copy-start.2 = (bf16[1,256,2048]{2,1,0:T(8,128)(2,1)S(1)}, bf16[1,256,2048]{2,1,0:T(8,128)(2,1)}, u32[]{:S(2)}) copy-start(bf16[1,256,2048]{2,1,0:T(8,128)(2,1)} %param.16) | copy-start | bytes 3145732
  6.5 32.7 %copy-start.11 = (f32[2048]{0:T(1024)S(1)}, f32[2048]{0:T(1024)}, u32[]{:S(2)}) copy-start(f32[2048]{0:T(1024)} %param.17) | copy-start | bytes 24580
  6.5 32.7 %all-gather.4.cloned.1.call-start = ((), (), s32[]{:S(2)}) async-start(), calls=%async_computation.2 | async-start | bytes 3538944 | tf_op jit(solution)/shard_map/all_gather | solution.py:18
  8.5 102.7 %all-gather.6.cloned.1.call-start = ((), (), s32[]{:S(2)}) async-start(), calls=%async_computation.3 | async-start | bytes 7798784 | tf_op jit(solution)/shard_map/all_gather | solution.py:18
  41.6 2.1 copy-start.7
  41.6 2.2 copy-start.8
  41.7 3.2 %copy-start.3 = (bf16[64,192]{1,0:T(8,128)(2,1)S(1)}, bf16[64,192]{1,0:T(8,128)(2,1)}, u32[]{:S(2)}) copy-start(bf16[64,192]{1,0:T(8,128)(2,1)} %param.23) | copy-start | bytes 73732
  41.7 8.7 %copy-start.5 = (bf16[32,128]{1,0:T(8,128)(2,1)S(1)}, bf16[32,128]{1,0:T(8,128)(2,1)}, u32[]{:S(2)}) copy-start(bf16[32,128]{1,0:T(8,128)(2,1)} %param.24) | copy-start | bytes 24580
  41.7 22.5 %copy-start.6 = (bf16[32,128]{1,0:T(8,128)(2,1)S(1)}, bf16[32,128]{1,0:T(8,128)(2,1)}, u32[]{:S(2)}) copy-start(bf16[32,128]{1,0:T(8,128)(2,1)} %param.25) | copy-start | bytes 24580
  45.6 70.2 %all-to-all-start = ((bf16[8,64,192]{2,1,0:T(8,128)(2,1)}), bf16[8,64,192]{2,1,0:T(8,128)(2,1)}, u32[]{:S(2)}, u32[]{:S(2)}) async-start(bf16[8,64,192]{2,1,0:T(8,128)(2,1)} %broadcast_in_dim.11), calls=%async_computation | async-start | bytes 524288 | tf_op jit(solution)/shard_map/all_to_all | solution.py:29
  49.6 162.7 %all-gather.8.cloned.1.call-start = ((), (), s32[]{:S(2)}) async-start(), calls=%async_computation.4 | async-start | bytes 8454144 | tf_op jit(solution)/shard_map/all_gather | solution.py:163
  115.8 3.8 %copy-start.9 = (f32[192]{0:T(256)S(1)}, f32[192]{0:T(256)}, u32[]{:S(2)}) copy-start(f32[192]{0:T(256)} %param.27) | copy-start | bytes 2308
  119.6 0.7 copy-start.10
  130.4 1.3 copy-start.1
  137.7 1.3 copy-start.1
  145.1 1.3 copy-start.1
  152.4 1.3 copy-start.1
  159.8 1.3 copy-start.1
  167.1 1.3 copy-start.1
  174.4 1.4 copy-start.1
  181.8 1.3 copy-start.1
  209.7 2.2 copy-start.4
Sparse Core Ops, SparseCore 0:
  9.0 30.1 all-gather.3
  44.9 66.1 all-gather.5
  114.2 69.2 all-gather.7
where the time goes:
time: 226 us
  waiting for transfers between devices  62.1 us (27%)
  matrix products  60.5 us (27%)
  blocking collectives  48.9 us (22%)
  other arithmetic  22.3 us (10%)
  between operations  13.4 us (6%)
  local copies, waits for them, and re-layouts  8.96 us (4%)
  loops' own time  5.21 us (2%)
  starting transfers between devices  4.13 us (2%)
    all_gather x2, waiting for transfers between devices, in_one_piece(): lax.all_gather(both, axis, axis=dim, tiled=True)  61.4 us
    dot_general x8, matrix products, one_block(): jnp.einsum('hqk,khd->qhd', weights, value_heads, preferred_element_type=j...  22.6 us
    all_to_all x1, blocking collectives, per_device(): lax.all_to_all(attended, 'sp', split_axis=0, concat_axis=1, tiled=True)  22.2 us
    dot_general x8, matrix products, one_block(): jnp.einsum('qhd,khd->hqk', query_block, key_heads, preferred_element_type...  15.7 us
    all_gather x1, blocking collectives, per_device(): lax.all_gather(w_key_up, 'dp', axis=0, tiled=True)  13.8 us
    all_gather x1, blocking collectives, per_device(): lax.all_gather(w_value_up, 'dp', axis=0, tiled=True)  12.9 us
    dot_general x2, matrix products, single_fold(): return jnp.dot(inputs, piece, preferred_element_type=jnp.float32)  10.5 us
    reduce_sum x8, other arithmetic, one_block(): weights = jax.nn.softmax(scores, axis=-1).astype(jnp.bfloat16)  10.2 us
  transfers between devices with their start and end apart: 4, of which 2 were waited for; matrix products, arithmetic and copies ran while one was open for 34% of the time, Pallas kernels for 0%

commit v1 on v0

--- a/solution.py
+++ b/solution.py
@@ -7,6 +7,13 @@
 EPS = 1e-06
 THETA = 10000.0
 NEG_BIG = -1e30
+
+
+def fill_the_seats_all(original):
+    mixed_arr = lax.axis_size("dp")
+    local_out = jnp.stack([original] * mixed_arr, axis=0)
+    aux = lax.all_to_all(local_out, "dp", 0, 0)
+    return jnp.concatenate(aux, axis=0)
 
 
 def in_one_piece(arrays, axis, dim, along):
@@ -149,10 +156,7 @@
     query_total = single_fold(every_q, gathered_copies(w_query_up, "dp", 0))
     key_total, value_total = double_fold(
         every_kv,
-        (
-            lax.all_gather(w_key_up, "dp", axis=0, tiled=True),
-            lax.all_gather(w_value_up, "dp", axis=0, tiled=True),
-        ),
+        (fill_the_seats_all(w_key_up), lax.all_gather(w_value_up, "dp", axis=0, tiled=True)),
     )
     queries = make_queries(query_total, positions, query_gain, head_count, rope_width)
     keys = make_keys(key_total, every_rope, positions, key_gain, head_count)

time: 226 us -> 238 us (1.053)
  waiting for transfers between devices: 62.1 us -> 81 us
  blocking collectives: 48.9 us -> 35.3 us
  starting transfers between devices: 4.13 us -> 7.69 us
    all_gather x2, waiting for transfers between devices: 61.4 us -> 75.4 us  [in_one_piece(): lax.all_gather(both, axis, axis=dim, tiled=True)]
    all_gather x1 -> x0, blocking collectives: 13.8 us -> none  [per_device(): lax.all_gather(w_key_up, 'dp', axis=0, tiled=True)]
    all_to_all x1, waiting for transfers between devices: 0.01 us -> 4.92 us  [sent_to_all(): return lax.all_to_all(copies, axis, split_axis=0, concat_axis=0, tiled=True)]
    all_to_all x0 -> x1, starting transfers between devices: none -> 3.35 us  [fill_the_seats_all(): aux = lax.all_to_all(local_out, 'dp', 0, 0)]
  transfers between devices with their start and end apart: 4 -> 5, of which waited for: 2 -> 3; matrix products, arithmetic and copies ran while one was open for 34% -> 33% of each run, Pallas kernels for 0% -> 0%
where the time goes in v1:
time: 238 us; the launch traced here: 237 us
  waiting for transfers between devices  81 us (34%)
  matrix products  60.4 us (25%)
  blocking collectives  35.3 us (15%)
  other arithmetic  22.3 us (9%)
  between operations  13.4 us (6%)
  local copies, waits for them, and re-layouts  10.9 us (5%)
  starting transfers between devices  7.69 us (3%)
  loops' own time  5.54 us (2%)
    all_gather x2, waiting for transfers between devices, in_one_piece(): lax.all_gather(both, axis, axis=dim, tiled=True)  75.4 us
    dot_general x8, matrix products, one_block(): jnp.einsum('hqk,khd->qhd', weights, value_heads, preferred_element_type=j...  22.6 us
    all_to_all x1, blocking collectives, per_device(): lax.all_to_all(attended, 'sp', split_axis=0, concat_axis=1, tiled=True)  21.8 us
    dot_general x8, matrix products, one_block(): jnp.einsum('qhd,khd->hqk', query_block, key_heads, preferred_element_type...  15.7 us
    all_gather x1, blocking collectives, per_device(): lax.all_gather(w_value_up, 'dp', axis=0, tiled=True)  13.5 us
    dot_general x2, matrix products, single_fold(): return jnp.dot(inputs, piece, preferred_element_type=jnp.float32)  10.5 us
    reduce_sum x8, other arithmetic, one_block(): weights = jax.nn.softmax(scores, axis=-1).astype(jnp.bfloat16)  10.2 us
    another operation x1, loops' own time, attend(): lax.map(one_block, (query_blocks, jnp.arange(length // block_rows)))  5.54 us
  transfers between devices with their start and end apart: 5, of which 3 were waited for; matrix products, arithmetic and copies ran while one was open for 33% of the time, Pallas kernels for 0%

profile of v1, /device:TPU:0, one launch (start us, length us, event | category | flops | bytes accessed | tf_op | source)
XLA Modules:
  0.0 236.6 jit_solution(13221884968214474306)
XLA Ops:
  6.5 1.9 pad_maximum_fusion.4
  8.5 1.5 fusion.17
  10.0 1.7 convolution_convert_fusion.2
  11.9 27.3 %all-gather.4.cloned.1.call-done = bf16[2048,768]{1,0:T(8,128)(2,1)} async-done(((bf16[256,768]{1,0:T(8,128)(2,1)}), bf16[2048,768]{1,0:T(8,128)(2,1)}) %all-gather.4.cloned.1.call-update) | async-done | bytes 3145744 | tf_op jit(solution)/shard_map/all_gather | solution.py:25
  39.2 2.4 %multiply_reduce_fusion.2 = (f32[256]{0:T(256)S(1)}, f32[256,512]{1,0:T(8,128)S(1)}) fusion(bf16[2048,768]{1,0:T(8,128)(2,1)} %all-gather.4.cloned.1.call-done, bf16[1,256,2048]{2,1,0:T(8,128)(2,1)S(1)} %copy-done.2, f32[2048]{0:T(1024)S(1)} %copy-done.10, f32[256]{0:T(256)S(1)} %add_rsqrt_fusion.5), kind=kOutput, calls=%fused_computation.61 | convolution fusion | flops 539229952 | bytes 3680256 | tf_op jit(solution)/shard_map/dot_general | solution.py:93
  41.7 1.9 multiply_reduce_fusion.3
  44.0 0.8 pad_maximum_fusion.3
  44.8 0.6 stack.2
  45.5 3.3 %all-to-all-start.1 = ((bf16[8,32,128]{2,1,0:T(8,128)(2,1)}), bf16[8,32,128]{2,1,0:T(8,128)(2,1)S(1)}, u32[]{:S(2)}, u32[]{:S(2)}) async-start(bf16[8,32,128]{2,1,0:T(8,128)(2,1)} %stack.2), calls=%async_computation.1 | async-start | bytes 131072 | tf_op jit(solution)/shard_map/all_to_all | solution.py:15
  48.9 0.7 all-gather.8.cloned.1.call-update
  49.6 13.5 %all_gather.14 = bf16[256,128]{1,0:T(8,128)(2,1)S(1)} all-gather(bf16[32,128]{1,0:T(8,128)(2,1)S(1)} %copy-done.5), channel_id=1, replica_groups=mesh['sp'=16,'dp'=8] {'dp'}, dimensions={0}, use_global_device_ids=true | all-gather | bytes 73728 | tf_op jit(solution)/shard_map/all_gather | solution.py:159
  63.1 48.1 %all-gather.6.cloned.1.call-done = bf16[4096,832]{1,0:T(8,128)(2,1)} async-done(((bf16[256,832]{1,0:T(8,128)(2,1)}), bf16[4096,832]{1,0:T(8,128)(2,1)}) %all-gather.6.cloned.1.call-update) | async-done | bytes 6815760 | tf_op jit(solution)/shard_map/all_gather | solution.py:25
  111.2 1.4 fusion.26
  112.5 0.6 copy.41
  113.1 1.5 broadcast_in_dim.11
  114.6 4.3 %all-to-all-start = ((bf16[8,64,192]{2,1,0:T(8,128)(2,1)}), bf16[8,64,192]{2,1,0:T(8,128)(2,1)}, u32[]{:S(2)}, u32[]{:S(2)}) async-start(bf16[8,64,192]{2,1,0:T(8,128)(2,1)} %broadcast_in_dim.11), calls=%async_computation | async-start | bytes 524288 | tf_op jit(solution)/shard_map/all_to_all | solution.py:36
  118.9 2.4 %convolution_bitcast_fusion = f32[4096,1,128]{0,2,1:T(8,128)S(1)} fusion(bf16[256,128]{1,0:T(8,128)(2,1)S(1)} %bitcast.89, bf16[4096,832]{1,0:T(8,128)(2,1)} %all-gather.6.cloned.1.call-done), kind=kOutput, calls=%fused_computation.16 | convolution fusion | flops 268435456 | bytes 4259840 | tf_op jit(solution)/shard_map/dot_general | solution.py:93
  121.3 0.3 multiply_reduce_fusion
  121.6 4.9 %all-to-all-done = bf16[8,64,192]{2,1,0:T(8,128)(2,1)} async-done(((bf16[8,64,192]{2,1,0:T(8,128)(2,1)}), bf16[8,64,192]{2,1,0:T(8,128)(2,1)}, u32[]{:S(2)}, u32[]{:S(2)}) %all-to-all-start) | async-done | bytes 196640 | tf_op jit(solution)/shard_map/all_to_all | solution.py:36
  126.5 3.8 %multiply_reduce_fusion.1 = (f32[4096]{0:T(1024)S(1)}, f32[4096,192]{0,1:T(8,128)S(1)}) fusion(bf16[512,192]{1,0:T(8,128)(2,1)} %bitcast.2, bf16[4096,832]{1,0:T(8,128)(2,1)} %all-gather.6.cloned.1.call-done), kind=kOutput, calls=%fused_computation.25 | convolution fusion | flops 806875136 | bytes 7618560 | tf_op jit(solution)/shard_map/dot_general | solution.py:88
  130.3 0.5 multiply_multiply_fusion
  130.9 0.5 multiply_bitcast_fusion
  131.6 2.5 %subtract_convert_fusion = (bf16[4096,1,32]{0,2,1:T(8,128)(2,1)S(1)}, bf16[4096,1,32]{0,2,1:T(8,128)(2,1)S(1)}, bf16[4096,1,32]{0,2,1:T(8,128)(2,1)S(1)}, bf16[4096,1,32]{0,2,1:T(8,128)(2,1)S(1)}) fusion(f32[4096,1,192]{0,2,1:T(8,128)S(1)} %multiply_multiply_fusion, f32[32]{0:T(128)S(1)} %multiply_power_fusion, f32[4096,1,192]{0,2,1:T(8,128)S(1)} %multiply_bitcast_fusion), kind=kLoop, calls=%fused_computation.54 | loop fusion | flops 2228224 | bytes 3145856 | tf_op jit(solution)/shard_map/convert.5
  134.5 3.3 %fusion.12 = bf16[4096,1,128]{2,0,1:T(8,128)(2,1)} fusion(bf16[256,128]{1,0:T(8,128)(2,1)S(1)} %all_gather.14, bf16[4096,832]{1,0:T(8,128)(2,1)} %all-gather.6.cloned.1.call-done), kind=kOutput, calls=%fused_computation.18 | convolution fusion | flops 268959744 | bytes 3211264 | tf_op jit(solution)/shard_map/dot_general | solution.py:94
  137.8 59.6 %while.11 = (s32[]{:T(128)}, bf16[8,512,1,128]{3,1,2,0:T(8,128)(2,1)}, s32[8]{0:T(128)S(1)}, bf16[8,512,1,192]{1,3,2,0:T(8,128)(2,1)S(1)}, bf16[4096,1,192]{0,2,...) while((s32[]{:T(128)}, bf16[8,512,1,128]{3,1,2,0:T(8,128)(2,1)}, ...), condition=%wide.region_8.9_spmd.clone, body=%wide.region_5.8_spmd.clone.sunk | while | flops 1361116672 | bytes 32324240 | solution.py:121
  137.8 0.6 dynamic_slice.19
  139.2 2.0 fusion.46
  141.1 1.3 fusion.47
  142.4 2.8 %fusion.48 = bf16[8,512,1,128]{3,1,2,0:T(8,128)(2,1)} fusion(bf16[8,512,1,128]{3,1,2,0:T(8,128)(2,1)} %get-tuple-element.141, s32[]{:T(128)} %get-tuple-element.140, f32[512,4096]{1,0:T(8,128)S(1)} %get-tuple-element.130, f32[512]{0:T(512)S(1)} %fusion.47, f32[512]{0:T(512)S(1)} %get-tuple-element.131, bf16[4096,1,128]{2,0,1:T(8,128)(2,1)S(1)} %copy-done.1), kind=kOutput, calls=%fused_computation.10.clone.1 | convolution fusion | flops 543227904 | bytes 9572864 | tf_op jit(solution)/shard_map/while/body/eval_jaxpr/hqk,khd->qhd/dot_general | solution.py:117
  145.2 0.6 dynamic_slice.19
  146.6 2.0 fusion.46
  148.5 1.3 fusion.47
  149.8 2.8 %fusion.48 = bf16[8,512,1,128]{3,1,2,0:T(8,128)(2,1)} fusion(bf16[8,512,1,128]{3,1,2,0:T(8,128)(2,1)} %get-tuple-element.141, s32[]{:T(128)} %get-tuple-element.140, f32[512,4096]{1,0:T(8,128)S(1)} %get-tuple-element.130, f32[512]{0:T(512)S(1)} %fusion.47, f32[512]{0:T(512)S(1)} %get-tuple-element.131, bf16[4096,1,128]{2,0,1:T(8,128)(2,1)S(1)} %copy-done.1), kind=kOutput, calls=%fused_computation.10.clone.1 | convolution fusion | flops 543227904 | bytes 9572864 | tf_op jit(solution)/shard_map/while/body/eval_jaxpr/hqk,khd->qhd/dot_general | solution.py:117
  152.6 0.6 dynamic_slice.19
  154.0 2.0 fusion.46
  155.9 1.3 fusion.47
  157.2 2.8 %fusion.48 = bf16[8,512,1,128]{3,1,2,0:T(8,128)(2,1)} fusion(bf16[8,512,1,128]{3,1,2,0:T(8,128)(2,1)} %get-tuple-element.141, s32[]{:T(128)} %get-tuple-element.140, f32[512,4096]{1,0:T(8,128)S(1)} %get-tuple-element.130, f32[512]{0:T(512)S(1)} %fusion.47, f32[512]{0:T(512)S(1)} %get-tuple-element.131, bf16[4096,1,128]{2,0,1:T(8,128)(2,1)S(1)} %copy-done.1), kind=kOutput, calls=%fused_computation.10.clone.1 | convolution fusion | flops 543227904 | bytes 9572864 | tf_op jit(solution)/shard_map/while/body/eval_jaxpr/hqk,khd->qhd/dot_general | solution.py:117
  160.1 0.6 dynamic_slice.19
  161.4 2.0 fusion.46
  163.3 1.3 fusion.47
  164.6 0.3 copy-done.1
  164.9 2.8 %fusion.48 = bf16[8,512,1,128]{3,1,2,0:T(8,128)(2,1)} fusion(bf16[8,512,1,128]{3,1,2,0:T(8,128)(2,1)} %get-tuple-element.141, s32[]{:T(128)} %get-tuple-element.140, f32[512,4096]{1,0:T(8,128)S(1)} %get-tuple-element.130, f32[512]{0:T(512)S(1)} %fusion.47, f32[512]{0:T(512)S(1)} %get-tuple-element.131, bf16[4096,1,128]{2,0,1:T(8,128)(2,1)S(1)} %copy-done.1), kind=kOutput, calls=%fused_computation.10.clone.1 | convolution fusion | flops 543227904 | bytes 9572864 | tf_op jit(solution)/shard_map/while/body/eval_jaxpr/hqk,khd->qhd/dot_general | solution.py:117
  167.7 0.6 dynamic_slice.19
  169.0 2.0 fusion.46
  171.0 1.3 fusion.47
  172.4 2.8 %fusion.48 = bf16[8,512,1,128]{3,1,2,0:T(8,128)(2,1)} fusion(bf16[8,512,1,128]{3,1,2,0:T(8,128)(2,1)} %get-tuple-element.141, s32[]{:T(128)} %get-tuple-element.140, f32[512,4096]{1,0:T(8,128)S(1)} %get-tuple-element.130, f32[512]{0:T(512)S(1)} %fusion.47, f32[512]{0:T(512)S(1)} %get-tuple-element.131, bf16[4096,1,128]{2,0,1:T(8,128)(2,1)S(1)} %copy-done.1), kind=kOutput, calls=%fused_computation.10.clone.1 | convolution fusion | flops 543227904 | bytes 9572864 | tf_op jit(solution)/shard_map/while/body/eval_jaxpr/hqk,khd->qhd/dot_general | solution.py:117
  175.2 0.6 dynamic_slice.19
  176.5 2.0 fusion.46
  178.5 1.3 fusion.47
  179.8 2.8 %fusion.48 = bf16[8,512,1,128]{3,1,2,0:T(8,128)(2,1)} fusion(bf16[8,512,1,128]{3,1,2,0:T(8,128)(2,1)} %get-tuple-element.141, s32[]{:T(128)} %get-tuple-element.140, f32[512,4096]{1,0:T(8,128)S(1)} %get-tuple-element.130, f32[512]{0:T(512)S(1)} %fusion.47, f32[512]{0:T(512)S(1)} %get-tuple-element.131, bf16[4096,1,128]{2,0,1:T(8,128)(2,1)S(1)} %copy-done.1), kind=kOutput, calls=%fused_computation.10.clone.1 | convolution fusion | flops 543227904 | bytes 9572864 | tf_op jit(solution)/shard_map/while/body/eval_jaxpr/hqk,khd->qhd/dot_general | solution.py:117
  182.6 0.6 dynamic_slice.19
  183.9 2.0 fusion.46
  185.9 1.3 fusion.47
  187.2 2.8 %fusion.48 = bf16[8,512,1,128]{3,1,2,0:T(8,128)(2,1)} fusion(bf16[8,512,1,128]{3,1,2,0:T(8,128)(2,1)} %get-tuple-element.141, s32[]{:T(128)} %get-tuple-element.140, f32[512,4096]{1,0:T(8,128)S(1)} %get-tuple-element.130, f32[512]{0:T(512)S(1)} %fusion.47, f32[512]{0:T(512)S(1)} %get-tuple-element.131, bf16[4096,1,128]{2,0,1:T(8,128)(2,1)S(1)} %copy-done.1), kind=kOutput, calls=%fused_computation.10.clone.1 | convolution fusion | flops 543227904 | bytes 9572864 | tf_op jit(solution)/shard_map/while/body/eval_jaxpr/hqk,khd->qhd/dot_general | solution.py:117
  190.0 0.6 dynamic_slice.19
  191.3 2.0 fusion.46
  193.3 1.3 fusion.47
  194.6 2.8 %fusion.48 = bf16[8,512,1,128]{3,1,2,0:T(8,128)(2,1)} fusion(bf16[8,512,1,128]{3,1,2,0:T(8,128)(2,1)} %get-tuple-element.141, s32[]{:T(128)} %get-tuple-element.140, f32[512,4096]{1,0:T(8,128)S(1)} %get-tuple-element.130, f32[512]{0:T(512)S(1)} %fusion.47, f32[512]{0:T(512)S(1)} %get-tuple-element.131, bf16[4096,1,128]{2,0,1:T(8,128)(2,1)S(1)} %copy-done.1), kind=kOutput, calls=%fused_computation.10.clone.1 | convolution fusion | flops 543227904 | bytes 9572864 | tf_op jit(solution)/shard_map/while/body/eval_jaxpr/hqk,khd->qhd/dot_general | solution.py:117
  197.4 21.8 %all_to_all.23 = bf16[16,256,128]{2,1,0:T(8,128)(2,1)S(1)} all-to-all(bf16[16,256,128]{2,1,0:T(8,128)(2,1)} %bitcast.8), channel_id=1, replica_groups=mesh['sp'=16,'dp'=8] {'sp'}, dimensions={0} | all-to-all | bytes 2097152 | tf_op jit(solution)/shard_map/all_to_all | solution.py:165
  219.2 1.6 convert_bitcast_fusion
  220.8 1.9 copy.42
  222.7 0.3 fusion.16
  223.0 0.3 fusion.23
  223.4 6.7 %fusion.15 = bf16[1,256,2048]{2,1,0:T(8,128)(2,1)} fusion(bf16[256,2048]{0,1:T(8,128)(2,1)S(1)} %fusion.23, bf16[2048,2048]{1,0:T(8,128)(2,1)} %all-gather.8.cloned.1.call-done), kind=kOutput, calls=%fused_computation.31 | convolution fusion | flops 2148007936 | bytes 10485760 | tf_op jit(solution)/shard_map/dot_general | solution.py:88
  (69 shorter events, 1.5 us)
Async XLA Ops:
  6.5 3.5 %copy-start = (bf16[2048,64]{0,1:T(8,128)(2,1)S(1)}, bf16[2048,64]{0,1:T(8,128)(2,1)}, u32[]{:S(2)}) copy-start(bf16[2048,64]{0,1:T(8,128)(2,1)} %param.20) | copy-start | bytes 786436
  6.5 32.7 %copy-start.2 = (bf16[1,256,2048]{2,1,0:T(8,128)(2,1)S(1)}, bf16[1,256,2048]{2,1,0:T(8,128)(2,1)}, u32[]{:S(2)}) copy-start(bf16[1,256,2048]{2,1,0:T(8,128)(2,1)} %param.16) | copy-start | bytes 3145732
  6.5 32.7 %copy-start.10 = (f32[2048]{0:T(1024)S(1)}, f32[2048]{0:T(1024)}, u32[]{:S(2)}) copy-start(f32[2048]{0:T(1024)} %param.17) | copy-start | bytes 24580
  6.5 32.7 %all-gather.4.cloned.1.call-start = ((), (), s32[]{:S(2)}) async-start(), calls=%async_computation.3 | async-start | bytes 3538944 | tf_op jit(solution)/shard_map/all_gather | solution.py:25
  8.5 102.7 %all-gather.6.cloned.1.call-start = ((), (), s32[]{:S(2)}) async-start(), calls=%async_computation.4 | async-start | bytes 7798784 | tf_op jit(solution)/shard_map/all_gather | solution.py:25
  41.6 2.1 copy-start.6
  41.6 2.2 copy-start.7
  41.7 3.2 %copy-start.4 = (bf16[32,128]{1,0:T(8,128)(2,1)S(1)}, bf16[32,128]{1,0:T(8,128)(2,1)}, u32[]{:S(2)}) copy-start(bf16[32,128]{1,0:T(8,128)(2,1)} %param.24) | copy-start | bytes 24580
  41.7 7.9 %copy-start.5 = (bf16[32,128]{1,0:T(8,128)(2,1)S(1)}, bf16[32,128]{1,0:T(8,128)(2,1)}, u32[]{:S(2)}) copy-start(bf16[32,128]{1,0:T(8,128)(2,1)} %param.25) | copy-start | bytes 24580
  45.5 67.7 %all-to-all-start.1 = ((bf16[8,32,128]{2,1,0:T(8,128)(2,1)}), bf16[8,32,128]{2,1,0:T(8,128)(2,1)S(1)}, u32[]{:S(2)}, u32[]{:S(2)}) async-start(bf16[8,32,128]{2,1,0:T(8,128)(2,1)} %stack.2), calls=%async_computation.1 | async-start | bytes 131072 | tf_op jit(solution)/shard_map/all_to_all | solution.py:15
  48.8 174.6 %all-gather.8.cloned.1.call-start = ((), (), s32[]{:S(2)}) async-start(), calls=%async_computation.5 | async-start | bytes 8454144 | tf_op jit(solution)/shard_map/all_gather | solution.py:167
  114.6 11.9 %all-to-all-start = ((bf16[8,64,192]{2,1,0:T(8,128)(2,1)}), bf16[8,64,192]{2,1,0:T(8,128)(2,1)}, u32[]{:S(2)}, u32[]{:S(2)}) async-start(bf16[8,64,192]{2,1,0:T(8,128)(2,1)} %broadcast_in_dim.11), calls=%async_computation | async-start | bytes 524288 | tf_op jit(solution)/shard_map/all_to_all | solution.py:36
  126.5 3.8 %copy-start.8 = (f32[192]{0:T(256)S(1)}, f32[192]{0:T(256)}, u32[]{:S(2)}) copy-start(f32[192]{0:T(256)} %param.27) | copy-start | bytes 2308
  130.3 0.7 copy-start.9
  141.1 1.3 copy-start.1
  148.5 1.3 copy-start.1
  155.9 1.3 copy-start.1
  163.3 1.5 copy-start.1
  171.0 1.4 copy-start.1
  178.5 1.3 copy-start.1
  185.9 1.3 copy-start.1
  193.3 1.3 copy-start.1
  220.8 2.2 copy-start.3
Sparse Core Ops, SparseCore 0:
  9.0 30.1 all-gather.3
  44.9 66.1 all-gather.5
  114.2 69.3 all-gather.7
